TPU v7x, 32 devices: a whole 2x2x4 slice. The times are simulated.
32 devices in a mesh: kv: 4 (over y, x), tp: 8 (over z, core).
Axes of the slice: x: 2, y: 2, z: 4, core: 2. Of those that a mesh axis runs over, the one named last changes fastest.
Arguments:
- resid: bfloat16 [32, 4096], P('tp', 'kv'), may hold values from -35 to 35
- attn_gain: bfloat16 [4096], replicated, may hold values from 0.099609375 to 1.8984375
- w_query_nope: bfloat16 [4096, 8192], P('kv', 'tp'), may hold values from -0.09375 to 0.09375
- w_query_rope: bfloat16 [4096, 4096], P('kv', 'tp'), may hold values from -0.09375 to 0.09375
- w_latent: bfloat16 [4096, 512], P('kv'), may hold values from -0.09375 to 0.09375
- w_key_rope: bfloat16 [4096, 64], replicated, may hold values from -0.09375 to 0.09375
- latent_gain: bfloat16 [512], replicated, may hold values from 0.099609375 to 1.8984375
- key_up: bfloat16 [512, 64, 128], P(None, 'tp'), may hold values from -0.5 to 0.5
- value_up: bfloat16 [512, 64, 128], P(None, 'tp'), may hold values from -0.25 to 0.25
- w_out: bfloat16 [8192, 4096], P('tp', 'kv'), may hold values from -4 to 4
- post_gain: bfloat16 [4096], replicated, may hold values from 0.099609375 to 1.8984375
- mlp_gain: bfloat16 [4096], replicated, may hold values from 0.099609375 to 1.8984375
- w_gate: bfloat16 [4096, 11008], P('kv', 'tp'), may hold values from -3 to 3
- w_up: bfloat16 [4096, 11008], P('kv', 'tp'), may hold values from -3 to 3
- w_down: bfloat16 [11008, 4096], P('tp', 'kv'), may hold values from -0.0546875 to 0.0546875
- cache_latent: bfloat16 [32, 2048, 512], P('tp', 'kv'), may hold values from -6 to 6
- cache_rope_key: bfloat16 [32, 2048, 64], P('tp', 'kv'), may hold values from -740 to 740
Outputs:
- next_resid: bfloat16 [32, 4096], P('tp', 'kv')
- new_latent: bfloat16 [32, 512], P('tp')
- new_rope_key: bfloat16 [32, 64], P('tp')
All inputs are finite; a program needn't handle non-finite values.
Results may differ from a plain program's by a relative error of at most 0.035.
Values may be sent and summed in bfloat16 or wider, within the bound.
A program may use at most 64 MiB of HBM per device.

v0:
```python
import functools

import jax
import jax.numpy as jnp
import numpy as np
from jax import lax
from jax.experimental import pallas as pl
from jax.experimental.pallas import tpu as pltpu
from jax.sharding import PartitionSpec as P

EPS = 1e-06
THETA = 10000.0


def rotate(vector, position):
    half_width = vector.shape[-1] // 2
    frequency = THETA ** (-jnp.arange(half_width, dtype=jnp.float32) / half_width)
    angles = jnp.asarray(position, jnp.float32) * frequency
    cos_table, sin_table = (jnp.cos(angles), jnp.sin(angles))
    lower_half, upper_half = (vector[..., :half_width], vector[..., half_width:])
    return jnp.concatenate(
        [
            lower_half * cos_table - upper_half * sin_table,
            lower_half * sin_table + upper_half * cos_table,
        ],
        axis=-1,
    )


def body(
    resid,
    attn_gain,
    w_query_nope,
    w_query_rope,
    w_latent,
    w_key_rope,
    latent_gain,
    key_up,
    value_up,
    w_out,
    post_gain,
    mlp_gain,
    w_gate,
    w_up,
    w_down,
    cache_latent,
    cache_rope_key,
):
    kv_count = lax.axis_size("kv")
    kv_index = lax.axis_index("kv")
    tp_index = lax.axis_index("tp")
    own_rows, width_dev = resid.shape
    model_width = width_dev * kv_count
    heads_dev = key_up.shape[1]
    pos_dev = cache_latent.shape[1]
    context = pos_dev * kv_count
    score_scale = (key_up.shape[2] + cache_rope_key.shape[2]) ** (-0.5)
    col_start = kv_index * width_dev
    row_start = tp_index * own_rows

    def block_of(vector):
        return lax.dynamic_slice_in_dim(vector, col_start, width_dev, 0).astype(jnp.float32)[
            None, :
        ]

    gathered = lax.all_gather(resid, "tp", axis=0, tiled=True)
    batch_rows = gathered.shape[0]
    gathered_float = gathered.astype(jnp.float32)
    normed_a = (gathered_float * block_of(attn_gain)).astype(jnp.bfloat16)
    own_normed = lax.dynamic_slice_in_dim(normed_a, row_start, own_rows, 0)
    key_rows = lax.dynamic_slice_in_dim(w_key_rope, col_start, width_dev, 0)
    q_nope_sum, q_rope_sum, latent_sum, key_sum, square_sum = (
        lax.psum(
            jnp.dot(normed_a, w_query_nope, preferred_element_type=jnp.float32).astype(
                jnp.bfloat16
            ),
            "kv",
        ).astype(jnp.float32),
        lax.psum(
            jnp.dot(normed_a, w_query_rope, preferred_element_type=jnp.float32).astype(
                jnp.bfloat16
            ),
            "kv",
        ).astype(jnp.float32),
        lax.psum(
            jnp.dot(own_normed, w_latent, preferred_element_type=jnp.float32).astype(jnp.bfloat16),
            "kv",
        ).astype(jnp.float32),
        lax.psum(
            jnp.dot(own_normed, key_rows, preferred_element_type=jnp.float32).astype(jnp.bfloat16),
            "kv",
        ).astype(jnp.float32),
        lax.psum(
            jnp.sum(gathered_float * gathered_float, axis=1).astype(jnp.bfloat16), "kv"
        ).astype(jnp.float32),
    )
    scale_in = lax.rsqrt(square_sum / model_width + EPS)[:, None]
    own_scale = lax.dynamic_slice_in_dim(scale_in, row_start, own_rows, 0)
    q_nope = (q_nope_sum * scale_in).astype(jnp.bfloat16).reshape(batch_rows, heads_dev, -1)
    q_rope = rotate((q_rope_sum * scale_in).reshape(batch_rows, heads_dev, -1), context).astype(
        jnp.bfloat16
    )
    new_latent = (
        latent_sum
        * lax.rsqrt(jnp.mean(latent_sum * latent_sum, axis=1, keepdims=True) + EPS)
        * latent_gain.astype(jnp.float32)[None, :]
    ).astype(jnp.bfloat16)
    new_rope_key = rotate(key_sum * own_scale, context).astype(jnp.bfloat16)
    q_lat = jnp.einsum("bhd,chd->bhc", q_nope, key_up, preferred_element_type=jnp.float32).astype(
        jnp.bfloat16
    )
    seq_lat, seq_rope = (
        lax.all_to_all(q_lat, "tp", split_axis=0, concat_axis=1, tiled=True),
        lax.all_to_all(q_rope, "tp", split_axis=0, concat_axis=1, tiled=True),
    )
    scores = (
        jnp.einsum("bhc,bpc->bhp", seq_lat, cache_latent, preferred_element_type=jnp.float32)
        + jnp.einsum("bhr,bpr->bhp", seq_rope, cache_rope_key, preferred_element_type=jnp.float32)
    ) * score_scale
    own_score = (
        jnp.einsum("bhc,bc->bh", seq_lat, new_latent, preferred_element_type=jnp.float32)
        + jnp.einsum("bhr,br->bh", seq_rope, new_rope_key, preferred_element_type=jnp.float32)
    ) * score_scale
    local_peak = jnp.maximum(jnp.max(scores, axis=2), own_score)
    peak = lax.pmax(local_peak, "kv")
    probs = jnp.exp(scores - peak[:, :, None])
    own_prob = jnp.exp(own_score - peak)
    totals = lax.psum(jnp.sum(probs, axis=2), "kv") + own_prob
    partial_value = jnp.einsum(
        "bhp,bpc->bhc", probs.astype(jnp.bfloat16), cache_latent, preferred_element_type=jnp.float32
    )
    summed = (
        lax.psum(partial_value.astype(jnp.bfloat16), "kv").astype(jnp.float32)
        + own_prob[:, :, None] * new_latent.astype(jnp.float32)[:, None, :]
    )
    o_lat = (summed / totals[:, :, None]).astype(jnp.bfloat16)
    head_lat = lax.all_to_all(o_lat, "tp", split_axis=1, concat_axis=0, tiled=True)
    o_heads = jnp.einsum(
        "bhc,che->bhe", head_lat, value_up, preferred_element_type=jnp.float32
    ).astype(jnp.bfloat16)
    o_flat = o_heads.reshape(batch_rows, -1)
    attended = lax.psum_scatter(
        jnp.dot(o_flat, w_out, preferred_element_type=jnp.float32).astype(jnp.bfloat16),
        "tp",
        scatter_dimension=0,
        tiled=True,
    ).astype(jnp.float32)
    post_square = lax.psum(jnp.sum(attended * attended, axis=1), "kv")
    post_part = attended * lax.rsqrt(post_square / model_width + EPS)[:, None] * block_of(post_gain)
    resid_mid = (resid.astype(jnp.float32) + post_part).astype(jnp.bfloat16)
    mid_rows = lax.all_gather(resid_mid, "tp", axis=0, tiled=True)
    mid_float = mid_rows.astype(jnp.float32)
    normed_m = (mid_float * block_of(mlp_gain)).astype(jnp.bfloat16)
    gate_part = jnp.dot(normed_m, w_gate, preferred_element_type=jnp.float32)
    up_part = jnp.dot(normed_m, w_up, preferred_element_type=jnp.float32)
    square_part = jnp.sum(mid_float * mid_float, axis=1)
    gate_sum, up_sum, mid_square = (
        lax.psum(gate_part.astype(jnp.bfloat16), "kv").astype(jnp.float32),
        lax.psum(up_part.astype(jnp.bfloat16), "kv").astype(jnp.float32),
        lax.psum(square_part.astype(jnp.bfloat16), "kv").astype(jnp.float32),
    )
    scale_mid = lax.rsqrt(mid_square / model_width + EPS)[:, None]
    hidden = (jax.nn.silu(gate_sum * scale_mid) * (up_sum * scale_mid)).astype(jnp.bfloat16)
    lowered = lax.psum_scatter(
        jnp.dot(hidden, w_down, preferred_element_type=jnp.float32).astype(jnp.bfloat16),
        "tp",
        scatter_dimension=0,
        tiled=True,
    ).astype(jnp.float32)
    next_resid = (resid_mid.astype(jnp.float32) + lowered).astype(jnp.bfloat16)
    return (next_resid, new_latent, new_rope_key)


F32 = jnp.float32
BF16 = jnp.bfloat16
MESH = pl.DeviceIdType.MESH


def dot_nt(a, b):
    return lax.dot_general(a, b, (((1,), (1,)), ((), ())), preferred_element_type=F32)


def lane_iota(shape):
    return lax.broadcasted_iota(jnp.int32, shape, len(shape) - 1)


def turn(v, cos, sin, half):
    width = v.shape[-1]
    low = lane_iota(v.shape) % (2 * half) < half
    swapped = jnp.where(low, pltpu.roll(v, width - half, 1), pltpu.roll(v, half, 1))
    return v * cos + swapped * sin


def layer_kernel(
    K, T, position_count,
    resid, attn_gain, latent_gain, post_gain, mlp_gain, cos_ref, sin_ref,
    h_wqn, h_wqr, h_wlat, h_wkr, h_ku, h_vu, h_wo, h_wg, h_wu, h_wd, h_cl, h_cr,
    out, out_lat, out_key,
    wqn, wqr, wlat, wkr, ku, vu, wo, wg, wu, wd, cl, cr,
    xbuf, xf, qs, qrv, sqs, sqr, lats, latr, qe, qbuf, accs, accr, mls, mlr,
    nls, nks, osend, obuf, ohs, h3, tall, es, er, ab, sqas, sqa, psq, attf, mids,
    gs, us, gr, ur, sqms, sqmr, hb, ls, lr, wide_ref, kus, vus,
    wsem, ssem, rsem,
):
    k = lax.axis_index("kv")
    t = lax.axis_index("tp")
    R, W = resid.shape
    D = W * K
    B = R * T
    LAT = h_wlat.shape[1]
    ROPE = h_wkr.shape[0]
    QN = h_wqn.shape[1]
    QR = h_wqr.shape[1]
    HD = QR // ROPE
    NOPE = QN // HD
    H = HD * T
    VD = h_vu.shape[1]
    half = ROPE // 2
    score_scale = (NOPE + ROPE) ** (-0.5)
    col = pl.ds(pl.multiple_of(k * W, 128), W)

    loads = {}
    pairs = [
        ("lat", h_wlat, wlat), ("kr", h_wkr.at[:, col], wkr), ("ku", h_ku, ku),
        ("qn", h_wqn, wqn), ("qr", h_wqr, wqr), ("vu", h_vu, vu), ("cl", h_cl, cl), ("cr", h_cr, cr),
        ("wo", h_wo, wo), ("wg", h_wg, wg), ("wu", h_wu, wu), ("wd", h_wd, wd),
    ]
    for i, (name, src, dst) in enumerate(pairs):
        loads[name] = pltpu.make_async_copy(src, dst, wsem.at[i])
        loads[name].start()

    others = [(a, b) for a in range(K) for b in range(T) if (a, b) != (0, 0)]
    tps = [(0, b) for b in range(1, T)]
    kvs = [(a, 0) for a in range(1, K)]

    def peer(off):
        return lax.rem(k + off[0], K), lax.rem(t + off[1], T)

    barrier = pltpu.get_barrier_semaphore()
    for off in others:
        pl.semaphore_signal(barrier, inc=1, device_id=peer(off), device_id_type=MESH)

    sent = []

    def send(src, dst, off):
        i = len(sent)
        copy = pltpu.make_async_remote_copy(
            src_ref=src, dst_ref=dst, send_sem=ssem.at[i], recv_sem=rsem.at[i],
            device_id=peer(off), device_id_type=MESH,
        )
        copy.start()
        sent.append(copy)
        return copy

    def arrive(copies):
        for copy in copies:
            copy.wait_recv()

    def dot(a, b):
        return jnp.dot(a, b[...], preferred_element_type=F32)

    def put_rows(ref, s, v):
        for c in range(ref.shape[0]):
            ref[c, pl.ds(s, R, stride=T), :] = v[:, c * 128:(c + 1) * 128]

    def rows(ref, s):
        return jnp.concatenate(
            [ref[c, pl.ds(s, R, stride=T), :] for c in range(ref.shape[0])], axis=1
        )

    def put_all(ref, v):
        for c in range(ref.shape[0]):
            ref[c] = v[:, c * 128:(c + 1) * 128]

    def all_rows(ref):
        return jnp.concatenate([ref[c] for c in range(ref.shape[0])], axis=1)

    gain_start = pl.multiple_of(k * (W // 128), W // 128)

    def gain_row(g):
        g = g.astype(F32)
        return jnp.concatenate([g[i:i + 1] for i in range(g.shape[0])], axis=1)

    def by_head(src, dst):
        n = src.shape[1]
        wide_ref[...] = src[...].astype(F32)
        for h in range(HD):
            dst[:, h * n:(h + 1) * n] = wide_ref[pl.ds(h, LAT, stride=HD), :].astype(BF16)

    xo = resid[...].astype(F32)
    xbuf[pl.ds(t, 1)] = resid[...][None]
    again = gain_row(attn_gain[pl.ds(gain_start, W // 128), :])
    own_normed = (xo * again).astype(BF16)
    loads["lat"].wait()
    loads["kr"].wait()
    lats[:, :LAT] = dot(own_normed, wlat)
    lats[:, LAT:LAT + ROPE] = dot_nt(own_normed, wkr[...])
    lats[:, LAT + ROPE:] = jnp.broadcast_to(
        jnp.sum(xo * xo, axis=1, keepdims=True), (R, lats.shape[1] - LAT - ROPE)
    )
    latr[pl.ds(k, 1)] = lats[...][None]
    pl.semaphore_wait(barrier, len(others))
    copies = [send(resid, xbuf.at[t], off) for off in tps]
    lat_copies = [send(lats, latr.at[k], off) for off in kvs]
    loads["ku"].wait()
    by_head(ku, kus)
    arrive(copies)
    for s in range(T):
        put_rows(xf, s, xbuf[s].astype(F32))
    x = all_rows(xf)
    normed = (x * again).astype(BF16)
    sqs[...] = jnp.broadcast_to(jnp.sum(x * x, axis=1, keepdims=True), (B, 128)).reshape(K, T, 128)
    loads["qn"].wait()
    qs[:, :, :QN] = dot(normed, wqn).reshape(K, T, QN).astype(BF16)
    loads["qr"].wait()
    qs[:, :, QN:] = dot(normed, wqr).reshape(K, T, QR).astype(BF16)
    copies = []
    for off in kvs:
        to = peer(off)[0]
        copies.append(send(qs.at[to], qrv.at[k], off))
        copies.append(send(sqs.at[to], sqr.at[k], off))
    qrv[pl.ds(k, 1)] = qs[pl.ds(k, 1)]
    sqr[pl.ds(k, 1)] = sqs[pl.ds(k, 1)]

    loads["vu"].wait()
    by_head(vu, vus)
    arrive(lat_copies)
    lat = sum(latr[s] for s in range(K))
    raw = lat[:, :LAT]
    new_lat = (
        raw * lax.rsqrt(jnp.mean(raw * raw, axis=1, keepdims=True) + EPS)
        * gain_row(latent_gain[...])
    ).astype(BF16)
    own_scale = lax.rsqrt(lat[:, LAT + ROPE:LAT + ROPE + 1] / D + EPS)
    tail = lat[:, LAT:]
    turned = turn(tail * own_scale, cos_ref[:, :tail.shape[1]], sin_ref[:, :tail.shape[1]], half)
    new_key = jnp.where(lane_iota(turned.shape) < ROPE, turned, 0.0).astype(BF16)
    out_lat[...] = new_lat
    out_key[...] = new_key[:, :ROPE]
    nls[...] = new_lat.astype(F32)
    nks[...] = new_key.astype(F32)

    arrive(copies)
    q = sum(qrv[s].astype(F32) for s in range(K))
    scale = lax.rsqrt(sum(sqr[s] for s in range(K))[:, :1] / D + EPS)
    q_nope = (q[:, :QN] * scale).astype(BF16).astype(F32)
    q_rope = turn(q[:, QN:] * scale, cos_ref[...], sin_ref[...], half).astype(BF16).astype(F32)

    def own_head(width, each):
        shape = (HD, width)
        return lane_iota(shape) // each == lax.broadcasted_iota(jnp.int32, shape, 0)

    def spread(v, each):
        mask = own_head(v.shape[1], each)
        return jnp.concatenate(
            [jnp.where(mask, jnp.broadcast_to(v[i:i + 1], mask.shape), 0.0) for i in range(T)], axis=0
        ).astype(BF16)

    RP = qe.shape[2] - LAT
    fold_shape = (QR, RP)
    fold = (
        lax.broadcasted_iota(jnp.int32, fold_shape, 0) % ROPE == lane_iota(fold_shape)
    ).astype(F32).astype(BF16)
    qe[:, :, LAT:] = jnp.dot(
        spread(q_rope, ROPE), fold, preferred_element_type=F32
    ).reshape(T, HD, RP).astype(BF16)
    qe[:, :, :LAT] = dot_nt(spread(q_nope, NOPE), kus[...]).reshape(T, HD, LAT).astype(BF16)
    copies = [send(qe.at[peer(off)[1]], qbuf.at[k, t], off) for off in tps]
    relayed = {off: [send(qe.at[t], qbuf.at[k, t], off)] for off in kvs}
    qbuf[pl.ds(k, 1), pl.ds(t, 1)] = qe[pl.ds(t, 1)][None]
    for away, copy in zip(tps, copies):
        copy.wait_recv()
        slot = qbuf.at[k, lax.rem(t + T - away[1], T)]
        for off in kvs:
            relayed[off].append(send(slot, slot, off))
    loads["cl"].wait()
    loads["cr"].wait()

    copies = []
    own_qb = None
    for off in [(0, 0)] + kvs:
        b = peer(off)[0]
        if off != (0, 0):
            arrive(relayed[(K - off[0], 0)])
        qb32 = qbuf[pl.ds(b, 1)][0].astype(F32).reshape(H, LAT + RP)
        qb = qb32.astype(BF16)
        keys = cl[pl.ds(b, 1)][0]
        scores = (
            dot_nt(qb[:, :LAT], keys) + jnp.dot(
                qb[:, LAT:LAT + ROPE], cr[pl.ds(b, 1)][0], preferred_element_type=F32
            )
        ) * score_scale
        m = jnp.max(scores, axis=1, keepdims=True)
        p = jnp.exp(scores - m)
        total = jnp.sum(p, axis=1, keepdims=True)
        acc = jnp.dot(p.astype(BF16), keys, preferred_element_type=F32).astype(BF16)
        ml = jnp.where(lane_iota((H, 128)) < 64, m, total)
        if off == (0, 0):
            own_qb = qb32
            accr[pl.ds(k, 1)] = acc[None]
            mlr[pl.ds(k, 1)] = ml[None]
        else:
            mls[off[0]] = ml
            accs[off[0]] = acc
            copies.append(send(mls.at[off[0]], mlr.at[k], off))
            copies.append(send(accs.at[off[0]], accr.at[k], off))
    nl = nls[pl.ds(k, 1), :]
    nk = nks[pl.ds(k, 1), :]
    own_score = (
        jnp.sum(own_qb[:, :LAT] * nl, axis=1, keepdims=True)
        + jnp.sum(own_qb[:, LAT:] * nk, axis=1, keepdims=True)
    ) * score_scale
    arrive(copies)
    peaks = [mlr[s][:, :1] for s in range(K)]
    peak = own_score
    for m in peaks:
        peak = jnp.maximum(peak, m)
    own_prob = jnp.exp(own_score - peak)
    total = own_prob
    summed = own_prob * nl
    for s in range(K):
        w = jnp.exp(peaks[s] - peak)
        total = total + w * mlr[s][:, 64:65]
        summed = summed + w * accr[s].astype(F32)
    osend[...] = (summed / total).reshape(T, HD, LAT).astype(BF16)
    copies = [send(osend.at[peer(off)[1]], obuf.at[t], off) for off in tps]
    obuf[pl.ds(t, 1)] = osend[pl.ds(t, 1)]
    arrive(copies)
    wide = dot(obuf[...].astype(F32).reshape(T * HD, LAT).astype(BF16), vus)
    mask = own_head(HD * VD, VD)
    for i in range(T):
        ohs[i:i + 1, :] = jnp.sum(
            jnp.where(mask, wide[i * HD:(i + 1) * HD], 0.0), axis=0, keepdims=True
        )
    h3[pl.ds(k, 1)] = ohs[...].astype(BF16)[None]
    copies = [send(h3.at[k], h3.at[k], off) for off in kvs]
    loads["wo"].wait()
    arrive(copies)
    put_all(tall, dot(h3[...].astype(F32).reshape(B, HD * VD).astype(BF16), wo))
    for s in range(T):
        es[s] = rows(tall, s).astype(BF16)
    copies = [send(es.at[peer(off)[1]], er.at[t], off) for off in tps]
    er[pl.ds(t, 1)] = es[pl.ds(t, 1)]
    arrive(copies)
    attended = sum(er[s].astype(F32) for s in range(T))
    sqas[...] = jnp.broadcast_to(jnp.sum(attended * attended, axis=1, keepdims=True), (R, 128))
    ab[pl.ds(t, 1)] = attended.astype(BF16)[None]
    copies = [send(sqas, sqa.at[k, t], off) for off in others]
    copies += [send(ab.at[t], ab.at[t], off) for off in tps]
    sqa[pl.ds(k, 1), pl.ds(t, 1)] = sqas[...][None, None]
    arrive(copies)
    for s in range(T):
        put_rows(attf, s, ab[s].astype(F32))
        psq[pl.ds(s, R, stride=T), :] = sum(sqa[j, s] for j in range(K))
    post_scale = lax.rsqrt(psq[...][:, :1] / D + EPS)
    mid = (
        x + all_rows(attf) * post_scale * gain_row(post_gain[pl.ds(gain_start, W // 128), :])
    ).astype(BF16).astype(F32)
    put_all(mids, mid)
    normed_m = (mid * gain_row(mlp_gain[pl.ds(gain_start, W // 128), :])).astype(BF16)
    sqms[...] = jnp.broadcast_to(
        jnp.sum(mid * mid, axis=1, keepdims=True), (B, 128)
    ).reshape(K, T, 128)
    FD = wg.shape[0]
    loads["wg"].wait()
    gs[...] = dot_nt(normed_m, wg[...]).reshape(K, T, FD).astype(BF16)
    copies = [send(gs.at[peer(off)[0]], gr.at[k], off) for off in kvs]
    copies += [send(sqms.at[peer(off)[0]], sqmr.at[k], off) for off in kvs]
    loads["wu"].wait()
    us[...] = dot_nt(normed_m, wu[...]).reshape(K, T, FD).astype(BF16)
    copies += [send(us.at[peer(off)[0]], ur.at[k], off) for off in kvs]
    gr[pl.ds(k, 1)] = gs[pl.ds(k, 1)]
    ur[pl.ds(k, 1)] = us[pl.ds(k, 1)]
    sqmr[pl.ds(k, 1)] = sqms[pl.ds(k, 1)]
    arrive(copies)
    mid_scale = lax.rsqrt(sum(sqmr[s] for s in range(K))[:, :1] / D + EPS)
    gate = sum(gr[s].astype(F32) for s in range(K)) * mid_scale
    up = sum(ur[s].astype(F32) for s in range(K)) * mid_scale
    hb[pl.ds(k, 1)] = (gate / (1.0 + jnp.exp(-gate)) * up).astype(BF16)[None]
    copies = [send(hb.at[k], hb.at[k], off) for off in kvs]
    loads["wd"].wait()
    arrive(copies)
    put_all(tall, dot(hb[...].astype(F32).reshape(B, FD).astype(BF16), wd))
    for s in range(T):
        ls[s] = rows(tall, s).astype(BF16)
    copies = [send(ls.at[peer(off)[1]], lr.at[t], off) for off in tps]
    lr[pl.ds(t, 1)] = ls[pl.ds(t, 1)]
    mid_own = rows(mids, t)
    arrive(copies)
    lowered = sum(lr[s].astype(F32) for s in range(T))
    out[...] = (mid_own + lowered).astype(BF16)
    for copy in sent:
        copy.wait_send()


def hand_over(a, b, c, a_out, b_out, c_out):
    for src, dst in ((a, a_out), (b, b_out), (c, c_out)):
        dst[...] = src[...]


def fused(
    resid, attn_gain, w_query_nope, w_query_rope, w_latent, w_key_rope, latent_gain, key_up,
    value_up, w_out, post_gain, mlp_gain, w_gate, w_up, w_down, cache_latent, cache_rope_key,
):
    K = lax.axis_size("kv")
    T = lax.axis_size("tp")
    R, W = resid.shape
    LAT, HD, _ = key_up.shape
    key_flat = key_up.reshape(LAT * HD, -1)
    value_flat = value_up.reshape(LAT * HD, -1)
    key_turned, rope_turned = w_key_rope.T, jnp.swapaxes(cache_rope_key, 1, 2)
    gate_turned, up_turned = w_gate.T, w_up.T
    ROPE = w_key_rope.shape[1]
    half = ROPE // 2
    context = cache_latent.shape[1] * K
    angle = context * THETA ** (-np.arange(half, dtype=np.float64) / half)
    cos = np.tile(np.cos(angle), 2 * HD)[None].astype(np.float32)
    sin = np.tile(np.concatenate([-np.sin(angle), np.sin(angle)]), HD)[None].astype(np.float32)
    B = R * T
    H = HD * T
    QN, QR, FD = w_query_nope.shape[1], w_query_rope.shape[1], w_gate.shape[1]
    HV = HD * value_up.shape[2]
    big = (w_query_nope, w_query_rope, w_latent, key_turned, key_flat, value_flat, w_out,
           gate_turned, up_turned, w_down, cache_latent, rope_turned)

    def held(a):
        return pltpu.VMEM((ROPE, W) if a is key_turned else a.shape, a.dtype)

    def bf(*shape):
        return pltpu.VMEM(shape, BF16)

    def fl(*shape):
        return pltpu.VMEM(shape, F32)

    LW = LAT + 128
    slabs = fl(W // 128, B, 128)
    scratch = [held(a) for a in big] + [
        bf(T, R, W), slabs, bf(K, T, QN + QR), bf(K, T, QN + QR), fl(K, T, 128), fl(K, T, 128),
        fl(R, LW), fl(K, R, LW), bf(T, HD, LW), bf(K, T, HD, LW), bf(K, H, LAT), bf(K, H, LAT),
        fl(K, H, 128), fl(K, H, 128), fl(R, LAT), fl(R, 128), bf(T, HD, LAT), bf(T, HD, LAT),
        fl(T, HV), bf(K, T, HV), slabs, bf(T, R, W), bf(T, R, W), bf(T, R, W),
        fl(R, 128), fl(K, T, R, 128), fl(B, 128), slabs, slabs,
        bf(K, T, FD), bf(K, T, FD), bf(K, T, FD), bf(K, T, FD), fl(K, T, 128), fl(K, T, 128),
        bf(K, T, FD), bf(T, R, W), bf(T, R, W),
        fl(*key_flat.shape), bf(LAT, QN), bf(LAT, HV),
    ]
    count = 10 * (K - 1) + 5 * (T - 1) + 2 * (K * T - 1) + 8
    vmem = pl.BlockSpec(memory_space=pltpu.VMEM)
    hbm = pl.BlockSpec(memory_space=pl.ANY)
    out_shape = (
        jax.ShapeDtypeStruct((R, W), BF16),
        jax.ShapeDtypeStruct((R, LAT), BF16),
        jax.ShapeDtypeStruct((R, ROPE), BF16),
    )
    made = pl.pallas_call(
        functools.partial(layer_kernel, K, T, context),
        out_shape=out_shape,
        in_specs=[vmem] * 7 + [hbm] * len(big),
        out_specs=(vmem, vmem, vmem),
        scratch_shapes=scratch + [
            pltpu.SemaphoreType.DMA((len(big),)),
            pltpu.SemaphoreType.DMA((count,)),
            pltpu.SemaphoreType.DMA((count,)),
        ],
        compiler_params=pltpu.CompilerParams(
            collective_id=0, has_side_effects=True, vmem_limit_bytes=60 * 1024 * 1024
        ),
    )(
        resid, *(g.reshape(-1, 128) for g in (attn_gain, latent_gain, post_gain, mlp_gain)),
        jnp.asarray(cos), jnp.asarray(sin), *big,
    )
    return pl.pallas_call(
        hand_over, out_shape=out_shape, in_specs=[vmem] * 3, out_specs=(vmem,) * 3
    )(*made)


def layer(*args):
    resid, key_up = args[0], args[7]
    kv, tp = lax.axis_size("kv"), lax.axis_size("tp")
    if resid.shape[0] == kv and key_up.shape[1] == 8 and tp == 8 and resid.shape[1] % 128 == 0:
        return fused(*args)
    return body(*args)


def solution(mesh):
    return jax.shard_map(
        layer,
        mesh=mesh,
        in_specs=(
            P("tp", "kv"),
            P(),
            P("kv", "tp"),
            P("kv", "tp"),
            P("kv", None),
            P(),
            P(),
            P(None, "tp", None),
            P(None, "tp", None),
            P("tp", "kv"),
            P(),
            P(),
            P("kv", "tp"),
            P("kv", "tp"),
            P("tp", "kv"),
            P("tp", "kv", None),
            P("tp", "kv", None),
        ),
        out_specs=(P("tp", "kv"), P("tp", None), P("tp", None)),
        check_vma=False,
    )
```

profile of v0, /device:TPU:0, one launch (start us, length us, event | category | flops | bytes accessed | tf_op | source)
XLA Modules:
  0.0 67.0 jit_solution(835924858568749507)
XLA Ops:
  0.6 65.0 %shard_map.202 = (bf16[4,1024]{1,0:T(4,128)(2,1)}, bf16[4,512]{1,0:T(4,128)(2,1)}, bf16[4,64]{1,0:T(4,128)(2,1)}) custom-call(bf16[4,1024]{1,0:T(4,128)(2,1)} %resid.1, bf16[32,128]{1,0:T(8,128)(2,1)} %bitcast.16, bf16[4,128]{1,0:T(4,128)(2,1)} %bitcast.19, bf16[32,128]{1,0:T(8,128)(2,1)} %bitcast.17, bf16[32,128]{1,0:T(8,128)(2,1)} %bitcast.18, ...), custom_call_target="tpu_custom_call" | custom-call | tf_op jit(solution)/shard_map/pallas_call | solution.py:555
  65.7 1.3 %shard_map.203 = (bf16[4,1024]{1,0:T(4,128)(2,1)}, bf16[4,512]{1,0:T(4,128)(2,1)}, bf16[4,64]{1,0:T(4,128)(2,1)}) custom-call(bf16[4,1024]{1,0:T(4,128)(2,1)} %get-tuple-element.6.a, bf16[4,512]{1,0:T(4,128)(2,1)} %get-tuple-element.7.b, bf16[4,64]{1,0:T(4,128)(2,1)} %get-tuple-element.8.c), custom_call_target="tpu_custom_call" | custom-call | tf_op jit(solution)/shard_map/pallas_call | solution.py:572
where the time goes:
time: 67.2 us; the launch traced here: 67 us
  Pallas kernels  66.3 us (99%)
    pallas_call x1, Pallas kernels, fused(): pl.pallas_call(functools.partial(layer_kernel, K, T, context), out_shape=...  65 us

commit v1 on v0

--- a/solution.py
+++ b/solution.py
@@ -191,20 +191,33 @@
     return v * cos + swapped * sin
 
 
+def flip(i, mask):
+    out, bit = i, 1
+    while bit <= mask:
+        if mask & bit:
+            out = out + bit - 2 * bit * lax.rem(lax.div(i, bit), 2)
+        bit *= 2
+    return out
+
+
+PHASES = ("x", "lat", "q", "sq", "qe", "rel", "acc", "ml", "o", "early", "h", "es", "ab", "gu", "sm", "hb", "ps", "ls")
+
+
 def layer_kernel(
-    K, T, position_count,
-    resid, attn_gain, latent_gain, post_gain, mlp_gain, cos_ref, sin_ref,
+    K, T,
+    h_x, h_ag, h_lg, h_pg, h_mg, h_cos, h_sin,
     h_wqn, h_wqr, h_wlat, h_wkr, h_ku, h_vu, h_wo, h_wg, h_wu, h_wd, h_cl, h_cr,
     out, out_lat, out_key,
+    ag, lg, pg, mg, cos_ref, sin_ref,
     wqn, wqr, wlat, wkr, ku, vu, wo, wg, wu, wd, cl, cr,
     xbuf, xf, qs, qrv, sqs, sqr, lats, latr, qe, qbuf, accs, accr, mls, mlr,
-    nls, nks, osend, obuf, ohs, h3, tall, es, er, ab, sqas, sqa, psq, attf, mids,
-    gs, us, gr, ur, sqms, sqmr, hb, ls, lr, wide_ref, kus, vus,
-    wsem, ssem, rsem,
+    nls, nks, osend, obuf, ohs, h3, es, er, ab, attf, tall,
+    eas, ear, easum, gus, gur, sms, smr, hb, psb, ls, lr, wide_ref, kus, vus,
+    lsem, ssem, rsem, qsem, relsem,
 ):
     k = lax.axis_index("kv")
     t = lax.axis_index("tp")
-    R, W = resid.shape
+    _, R, W = xbuf.shape
     D = W * K
     B = R * T
     LAT = h_wlat.shape[1]
@@ -218,43 +231,54 @@
     half = ROPE // 2
     score_scale = (NOPE + ROPE) ** (-0.5)
     col = pl.ds(pl.multiple_of(k * W, 128), W)
+    gain_rows = pl.ds(pl.multiple_of(k * (W // 128), W // 128), W // 128)
+
+    z, core = lax.div(t, 2), lax.rem(t, 2)
+    middle = lax.rem(lax.div(z + 1, 2), 2)
+    two, end = lax.rem(z + 2, 4), 3 - z
+    far = middle * two + (1 - middle) * end
+    mid = middle * end + (1 - middle) * two
+    near = flip(z, 1)
+    by_arrival = [flip(t, 1)] + [2 * zz + cc for zz in (near, mid, far) for cc in (core, 1 - core)]
+    tps = by_arrival[::-1]
+    kvs = [flip(k, m) for m in (3, 1, 2)]
+
+    barrier = pltpu.get_barrier_semaphore()
+    for kk, tt in [(kk, t) for kk in kvs] + [(k, tt) for tt in tps]:
+        pl.semaphore_signal(barrier, inc=1, device_id=(kk, tt), device_id_type=MESH)
 
     loads = {}
     pairs = [
-        ("lat", h_wlat, wlat), ("kr", h_wkr.at[:, col], wkr), ("ku", h_ku, ku),
-        ("qn", h_wqn, wqn), ("qr", h_wqr, wqr), ("vu", h_vu, vu), ("cl", h_cl, cl), ("cr", h_cr, cr),
-        ("wo", h_wo, wo), ("wg", h_wg, wg), ("wu", h_wu, wu), ("wd", h_wd, wd),
+        ("x", h_x, xbuf.at[t]), ("ag", h_ag.at[gain_rows], ag), ("lat", h_wlat, wlat),
+        ("kr", h_wkr.at[:, col], wkr), ("ku", h_ku, ku), ("qn", h_wqn, wqn), ("qr", h_wqr, wqr),
+        ("lg", h_lg, lg), ("cos", h_cos, cos_ref), ("sin", h_sin, sin_ref),
+        ("vu", h_vu, vu), ("cl", h_cl, cl), ("cr", h_cr, cr),
+        ("mg", h_mg.at[gain_rows], mg), ("pg", h_pg.at[gain_rows], pg),
+        ("wg", h_wg, wg), ("wu", h_wu, wu), ("wo", h_wo, wo), ("wd", h_wd, wd),
     ]
     for i, (name, src, dst) in enumerate(pairs):
-        loads[name] = pltpu.make_async_copy(src, dst, wsem.at[i])
+        loads[name] = pltpu.make_async_copy(src, dst, lsem.at[i])
         loads[name].start()
 
-    others = [(a, b) for a in range(K) for b in range(T) if (a, b) != (0, 0)]
-    tps = [(0, b) for b in range(1, T)]
-    kvs = [(a, 0) for a in range(1, K)]
-
-    def peer(off):
-        return lax.rem(k + off[0], K), lax.rem(t + off[1], T)
-
-    barrier = pltpu.get_barrier_semaphore()
-    for off in others:
-        pl.semaphore_signal(barrier, inc=1, device_id=peer(off), device_id_type=MESH)
-
-    sent = []
-
-    def send(src, dst, off):
-        i = len(sent)
-        copy = pltpu.make_async_remote_copy(
-            src_ref=src, dst_ref=dst, send_sem=ssem.at[i], recv_sem=rsem.at[i],
-            device_id=peer(off), device_id_type=MESH,
-        )
-        copy.start()
-        sent.append(copy)
-        return copy
-
-    def arrive(copies):
-        for copy in copies:
-            copy.wait_recv()
+    def send(phase, src, dst, to, landed=None):
+        i = PHASES.index(phase)
+        pltpu.make_async_remote_copy(
+            src_ref=src, dst_ref=dst, send_sem=ssem.at[i],
+            recv_sem=rsem.at[i] if landed is None else landed,
+            device_id=to, device_id_type=MESH,
+        ).start()
+
+    def settle(ref, sem):
+        pltpu.make_async_remote_copy(
+            src_ref=ref, dst_ref=ref, send_sem=sem, recv_sem=sem,
+            device_id=(k, tps[-1]), device_id_type=MESH,
+        ).wait_recv()
+
+    def arrive(phase, ref):
+        settle(ref, rsem.at[PHASES.index(phase)])
+
+    def left(phase, ref):
+        settle(ref, ssem.at[PHASES.index(phase)])
 
     def dot(a, b):
         return jnp.dot(a, b[...], preferred_element_type=F32)
@@ -275,10 +299,8 @@
     def all_rows(ref):
         return jnp.concatenate([ref[c] for c in range(ref.shape[0])], axis=1)
 
-    gain_start = pl.multiple_of(k * (W // 128), W // 128)
-
-    def gain_row(g):
-        g = g.astype(F32)
+    def gain_row(ref):
+        g = ref[...].astype(F32)
         return jnp.concatenate([g[i:i + 1] for i in range(g.shape[0])], axis=1)
 
     def by_head(src, dst):
@@ -287,9 +309,13 @@
         for h in range(HD):
             dst[:, h * n:(h + 1) * n] = wide_ref[pl.ds(h, LAT, stride=HD), :].astype(BF16)
 
-    xo = resid[...].astype(F32)
-    xbuf[pl.ds(t, 1)] = resid[...][None]
-    again = gain_row(attn_gain[pl.ds(gain_start, W // 128), :])
+    loads["x"].wait()
+    pl.semaphore_wait(barrier, len(tps) + len(kvs))
+    for tt in tps:
+        send("x", xbuf.at[t], xbuf.at[t], (k, tt))
+    xo = xbuf[pl.ds(t, 1)][0].astype(F32)
+    loads["ag"].wait()
+    again = gain_row(ag)
     own_normed = (xo * again).astype(BF16)
     loads["lat"].wait()
     loads["kr"].wait()
@@ -299,12 +325,11 @@
         jnp.sum(xo * xo, axis=1, keepdims=True), (R, lats.shape[1] - LAT - ROPE)
     )
     latr[pl.ds(k, 1)] = lats[...][None]
-    pl.semaphore_wait(barrier, len(others))
-    copies = [send(resid, xbuf.at[t], off) for off in tps]
-    lat_copies = [send(lats, latr.at[k], off) for off in kvs]
+    for kk in kvs:
+        send("lat", lats, latr.at[k], (kk, t))
     loads["ku"].wait()
     by_head(ku, kus)
-    arrive(copies)
+    arrive("x", xbuf.at[pl.ds(0, T - 1)])
     for s in range(T):
         put_rows(xf, s, xbuf[s].astype(F32))
     x = all_rows(xf)
@@ -314,22 +339,20 @@
     qs[:, :, :QN] = dot(normed, wqn).reshape(K, T, QN).astype(BF16)
     loads["qr"].wait()
     qs[:, :, QN:] = dot(normed, wqr).reshape(K, T, QR).astype(BF16)
-    copies = []
-    for off in kvs:
-        to = peer(off)[0]
-        copies.append(send(qs.at[to], qrv.at[k], off))
-        copies.append(send(sqs.at[to], sqr.at[k], off))
+    for kk in kvs:
+        send("q", qs.at[kk], qrv.at[k], (kk, t))
+        send("sq", sqs.at[kk], sqr.at[k], (kk, t))
     qrv[pl.ds(k, 1)] = qs[pl.ds(k, 1)]
     sqr[pl.ds(k, 1)] = sqs[pl.ds(k, 1)]
-
     loads["vu"].wait()
     by_head(vu, vus)
-    arrive(lat_copies)
+    for name in ("lg", "cos", "sin"):
+        loads[name].wait()
+    arrive("lat", latr.at[pl.ds(0, K - 1)])
     lat = sum(latr[s] for s in range(K))
     raw = lat[:, :LAT]
     new_lat = (
-        raw * lax.rsqrt(jnp.mean(raw * raw, axis=1, keepdims=True) + EPS)
-        * gain_row(latent_gain[...])
+        raw * lax.rsqrt(jnp.mean(raw * raw, axis=1, keepdims=True) + EPS) * gain_row(lg)
     ).astype(BF16)
     own_scale = lax.rsqrt(lat[:, LAT + ROPE:LAT + ROPE + 1] / D + EPS)
     tail = lat[:, LAT:]
@@ -340,9 +363,11 @@
     nls[...] = new_lat.astype(F32)
     nks[...] = new_key.astype(F32)
 
-    arrive(copies)
+    arrive("q", qrv.at[pl.ds(0, K - 1)])
+    arrive("sq", sqr.at[pl.ds(0, K - 1)])
     q = sum(qrv[s].astype(F32) for s in range(K))
-    scale = lax.rsqrt(sum(sqr[s] for s in range(K))[:, :1] / D + EPS)
+    square = sum(sqr[s] for s in range(K))[:, :1]
+    scale = lax.rsqrt(square / D + EPS)
     q_nope = (q[:, :QN] * scale).astype(BF16).astype(F32)
     q_rope = turn(q[:, QN:] * scale, cos_ref[...], sin_ref[...], half).astype(BF16).astype(F32)
 
@@ -365,23 +390,20 @@
         spread(q_rope, ROPE), fold, preferred_element_type=F32
     ).reshape(T, HD, RP).astype(BF16)
     qe[:, :, :LAT] = dot_nt(spread(q_nope, NOPE), kus[...]).reshape(T, HD, LAT).astype(BF16)
-    copies = [send(qe.at[peer(off)[1]], qbuf.at[k, t], off) for off in tps]
-    relayed = {off: [send(qe.at[t], qbuf.at[k, t], off)] for off in kvs}
+    for tt in tps:
+        send("qe", qe.at[tt], qbuf.at[k, t], (k, tt), qsem.at[t])
+    for i, kk in enumerate(kvs):
+        send("rel", qe.at[t], qbuf.at[k, t], (kk, t), relsem.at[i])
     qbuf[pl.ds(k, 1), pl.ds(t, 1)] = qe[pl.ds(t, 1)][None]
-    for away, copy in zip(tps, copies):
-        copy.wait_recv()
-        slot = qbuf.at[k, lax.rem(t + T - away[1], T)]
-        for off in kvs:
-            relayed[off].append(send(slot, slot, off))
+    for tt in by_arrival:
+        slot = qbuf.at[k, tt]
+        settle(slot, qsem.at[tt])
+        for i, kk in enumerate(kvs):
+            send("rel", slot, slot, (kk, t), relsem.at[i])
     loads["cl"].wait()
     loads["cr"].wait()
 
-    copies = []
-    own_qb = None
-    for off in [(0, 0)] + kvs:
-        b = peer(off)[0]
-        if off != (0, 0):
-            arrive(relayed[(K - off[0], 0)])
+    def attend(b):
         qb32 = qbuf[pl.ds(b, 1)][0].astype(F32).reshape(H, LAT + RP)
         qb = qb32.astype(BF16)
         keys = cl[pl.ds(b, 1)][0]
@@ -394,24 +416,31 @@
         p = jnp.exp(scores - m)
         total = jnp.sum(p, axis=1, keepdims=True)
         acc = jnp.dot(p.astype(BF16), keys, preferred_element_type=F32).astype(BF16)
-        ml = jnp.where(lane_iota((H, 128)) < 64, m, total)
-        if off == (0, 0):
-            own_qb = qb32
-            accr[pl.ds(k, 1)] = acc[None]
-            mlr[pl.ds(k, 1)] = ml[None]
-        else:
-            mls[off[0]] = ml
-            accs[off[0]] = acc
-            copies.append(send(mls.at[off[0]], mlr.at[k], off))
-            copies.append(send(accs.at[off[0]], accr.at[k], off))
+        turned_ml = jnp.where(lane_iota((H, 2 * H)) < H, m, total).T
+        return qb32, acc, turned_ml[:1], turned_ml[H:H + 1]
+
+    own_qb, acc, m_row, total_row = attend(k)
+    accr[pl.ds(k, 1)] = acc[None]
+    mlr[pl.ds(k, 1), 0:1, :H] = m_row[None]
+    mlr[pl.ds(k, 1), 1:2, :H] = total_row[None]
     nl = nls[pl.ds(k, 1), :]
     nk = nks[pl.ds(k, 1), :]
     own_score = (
         jnp.sum(own_qb[:, :LAT] * nl, axis=1, keepdims=True)
         + jnp.sum(own_qb[:, LAT:] * nk, axis=1, keepdims=True)
     ) * score_scale
-    arrive(copies)
-    peaks = [mlr[s][:, :1] for s in range(K)]
+    for i, kk in ((1, kvs[1]), (2, kvs[2]), (0, kvs[0])):
+        settle(qbuf.at[kk], relsem.at[i])
+        _, acc, m_row, total_row = attend(kk)
+        mls[i, 0:1, :H] = m_row
+        mls[i, 1:2, :H] = total_row
+        accs[i] = acc
+        send("acc", accs.at[i], accr.at[k], (kk, t))
+        send("ml", mls.at[i], mlr.at[k], (kk, t))
+    arrive("ml", mlr.at[pl.ds(0, K - 1)])
+    arrive("acc", accr.at[pl.ds(0, K - 1)])
+    columns = mlr[...].reshape(K * mlr.shape[1], mlr.shape[2]).T[:H]
+    peaks = [columns[:, 8 * s:8 * s + 1] for s in range(K)]
     peak = own_score
     for m in peaks:
         peak = jnp.maximum(peak, m)
@@ -420,12 +449,23 @@
     summed = own_prob * nl
     for s in range(K):
         w = jnp.exp(peaks[s] - peak)
-        total = total + w * mlr[s][:, 64:65]
+        total = total + w * columns[:, 8 * s + 1:8 * s + 2]
         summed = summed + w * accr[s].astype(F32)
     osend[...] = (summed / total).reshape(T, HD, LAT).astype(BF16)
-    copies = [send(osend.at[peer(off)[1]], obuf.at[t], off) for off in tps]
+    for tt in tps:
+        send("o", osend.at[tt], obuf.at[t], (k, tt))
     obuf[pl.ds(t, 1)] = osend[pl.ds(t, 1)]
-    arrive(copies)
+
+    FD = wg.shape[0]
+    loads["mg"].wait()
+    early = (all_rows(xf) * gain_row(mg)).astype(BF16)
+    for i, (name, w) in enumerate((("wg", wg), ("wu", wu))):
+        loads[name].wait()
+        eas[:, i] = dot_nt(early, w[...]).reshape(K, T, FD).astype(BF16)
+        for kk in kvs:
+            send("early", eas.at[kk, i], ear.at[k, i], (kk, t))
+    ear[pl.ds(k, 1)] = eas[pl.ds(k, 1)]
+    arrive("o", obuf.at[pl.ds(0, T - 1)])
     wide = dot(obuf[...].astype(F32).reshape(T * HD, LAT).astype(BF16), vus)
     mask = own_head(HD * VD, VD)
     for i in range(T):
@@ -433,64 +473,116 @@
             jnp.where(mask, wide[i * HD:(i + 1) * HD], 0.0), axis=0, keepdims=True
         )
     h3[pl.ds(k, 1)] = ohs[...].astype(BF16)[None]
-    copies = [send(h3.at[k], h3.at[k], off) for off in kvs]
+    for kk in kvs:
+        send("h", h3.at[k], h3.at[k], (kk, t))
     loads["wo"].wait()
-    arrive(copies)
-    put_all(tall, dot(h3[...].astype(F32).reshape(B, HD * VD).astype(BF16), wo))
-    for s in range(T):
-        es[s] = rows(tall, s).astype(BF16)
-    copies = [send(es.at[peer(off)[1]], er.at[t], off) for off in tps]
-    er[pl.ds(t, 1)] = es[pl.ds(t, 1)]
-    arrive(copies)
-    attended = sum(er[s].astype(F32) for s in range(T))
-    sqas[...] = jnp.broadcast_to(jnp.sum(attended * attended, axis=1, keepdims=True), (R, 128))
-    ab[pl.ds(t, 1)] = attended.astype(BF16)[None]
-    copies = [send(sqas, sqa.at[k, t], off) for off in others]
-    copies += [send(ab.at[t], ab.at[t], off) for off in tps]
-    sqa[pl.ds(k, 1), pl.ds(t, 1)] = sqas[...][None, None]
-    arrive(copies)
-    for s in range(T):
-        put_rows(attf, s, ab[s].astype(F32))
-        psq[pl.ds(s, R, stride=T), :] = sum(sqa[j, s] for j in range(K))
-    post_scale = lax.rsqrt(psq[...][:, :1] / D + EPS)
-    mid = (
-        x + all_rows(attf) * post_scale * gain_row(post_gain[pl.ds(gain_start, W // 128), :])
-    ).astype(BF16).astype(F32)
-    put_all(mids, mid)
-    normed_m = (mid * gain_row(mlp_gain[pl.ds(gain_start, W // 128), :])).astype(BF16)
-    sqms[...] = jnp.broadcast_to(
-        jnp.sum(mid * mid, axis=1, keepdims=True), (B, 128)
+    arrive("h", h3.at[pl.ds(0, K - 1)])
+    es[...] = dot(h3[...].astype(F32).reshape(B, HD * VD).astype(BF16), wo).reshape(K, T, W).astype(BF16)
+    first = (T - K) // 2
+    mine = t - first
+    owner = jnp.logical_and(mine >= 0, mine < K)
+    for i in range(K):
+        j = lax.rem(i + (K // 2) * (1 - lax.div(t, T // 2)), K)
+
+        @pl.when(mine != j)
+        def _():
+            send("es", es.at[j], er.at[t], (k, first + j))
+
+    arrive("early", ear.at[pl.ds(0, K - 1)])
+    easum[...] = sum(ear[s].astype(F32) for s in range(K))
+    loads["pg"].wait()
+
+    @pl.when(owner)
+    def _():
+        er[pl.ds(t, 1)] = es[pl.ds(mine, 1)]
+        arrive("es", er.at[pl.ds(0, T - 1)])
+        ab[pl.ds(mine, 1)] = sum(er[s].astype(F32) for s in range(T)).astype(BF16)[None]
+        for tt in tps:
+            send("ab", ab.at[mine], ab.at[mine], (k, tt))
+        arrive("ab", ab.at[pl.ds(0, K - 1)])
+
+    @pl.when(jnp.logical_not(owner))
+    def _():
+        arrive("ab", ab)
+
+    att = ab[...].astype(F32).reshape(B, W)
+    added = att * gain_row(pg)
+    late = (added * gain_row(mg)).astype(BF16)
+    gus[:, 0] = dot_nt(late, wg[...]).reshape(K, T, FD).astype(BF16)
+    for kk in kvs:
+        send("gu", gus.at[kk, 0], gur.at[k, 0], (kk, t))
+    gus[:, 1] = dot_nt(late, wu[...]).reshape(K, T, FD).astype(BF16)
+    for kk in kvs:
+        send("gu", gus.at[kk, 1], gur.at[k, 1], (kk, t))
+    lane = lane_iota((B, 128))
+    parts = (
+        jnp.sum(att * att, axis=1, keepdims=True),
+        jnp.sum(all_rows(xf) * added, axis=1, keepdims=True),
+        jnp.sum(added * added, axis=1, keepdims=True),
+    )
+    sms[...] = jnp.where(
+        lane < 32, parts[0], jnp.where(lane < 64, parts[1], parts[2])
     ).reshape(K, T, 128)
-    FD = wg.shape[0]
-    loads["wg"].wait()
-    gs[...] = dot_nt(normed_m, wg[...]).reshape(K, T, FD).astype(BF16)
-    copies = [send(gs.at[peer(off)[0]], gr.at[k], off) for off in kvs]
-    copies += [send(sqms.at[peer(off)[0]], sqmr.at[k], off) for off in kvs]
-    loads["wu"].wait()
-    us[...] = dot_nt(normed_m, wu[...]).reshape(K, T, FD).astype(BF16)
-    copies += [send(us.at[peer(off)[0]], ur.at[k], off) for off in kvs]
-    gr[pl.ds(k, 1)] = gs[pl.ds(k, 1)]
-    ur[pl.ds(k, 1)] = us[pl.ds(k, 1)]
-    sqmr[pl.ds(k, 1)] = sqms[pl.ds(k, 1)]
-    arrive(copies)
-    mid_scale = lax.rsqrt(sum(sqmr[s] for s in range(K))[:, :1] / D + EPS)
-    gate = sum(gr[s].astype(F32) for s in range(K)) * mid_scale
-    up = sum(ur[s].astype(F32) for s in range(K)) * mid_scale
+    for kk in kvs:
+        send("sm", sms.at[kk], smr.at[k], (kk, t))
+    gur[pl.ds(k, 1)] = gus[pl.ds(k, 1)]
+    smr[pl.ds(k, 1)] = sms[pl.ds(k, 1)]
+    put_all(attf, att)
+    arrive("sm", smr.at[pl.ds(0, K - 1)])
+    arrive("gu", gur.at[pl.ds(0, K - 1)])
+    sums = sum(smr[s] for s in range(K))
+    post_scale = lax.rsqrt(sums[:, :1] / D + EPS)
+    mid_square = square + post_scale * (2.0 * sums[:, 32:33] + post_scale * sums[:, 64:65])
+    mid_scale = lax.rsqrt(jnp.maximum(mid_square, 0.0) / D + EPS)
+    gate = (easum[0] + post_scale * sum(gur[s, 0].astype(F32) for s in range(K))) * mid_scale
+    up = (easum[1] + post_scale * sum(gur[s, 1].astype(F32) for s in range(K))) * mid_scale
     hb[pl.ds(k, 1)] = (gate / (1.0 + jnp.exp(-gate)) * up).astype(BF16)[None]
-    copies = [send(hb.at[k], hb.at[k], off) for off in kvs]
+    psb[pl.ds(k, 1)] = jnp.broadcast_to(post_scale, (T, 128))[None]
+    for kk in kvs:
+        send("hb", hb.at[k], hb.at[k], (kk, t))
+        send("ps", psb.at[k], psb.at[k], (kk, t))
     loads["wd"].wait()
-    arrive(copies)
+    arrive("hb", hb.at[pl.ds(0, K - 1)])
     put_all(tall, dot(hb[...].astype(F32).reshape(B, FD).astype(BF16), wd))
     for s in range(T):
         ls[s] = rows(tall, s).astype(BF16)
-    copies = [send(ls.at[peer(off)[1]], lr.at[t], off) for off in tps]
+    for tt in tps:
+        send("ls", ls.at[tt], lr.at[t], (k, tt))
     lr[pl.ds(t, 1)] = ls[pl.ds(t, 1)]
-    mid_own = rows(mids, t)
-    arrive(copies)
+    arrive("ps", psb.at[pl.ds(0, K - 1)])
+    own_post = psb[:, pl.ds(t, 1), :].reshape(K, 128)[:, :1]
+    mid_own = (
+        xbuf[pl.ds(t, 1)][0].astype(F32) + rows(attf, t) * own_post * gain_row(pg)
+    ).astype(BF16).astype(F32)
+    left("x", xbuf.at[pl.ds(0, T - 1)])
+    left("lat", latr.at[pl.ds(0, K - 1)])
+    left("q", qs.at[pl.ds(0, K - 1)])
+    left("sq", sqs.at[pl.ds(0, K - 1)])
+    left("qe", qe.at[pl.ds(0, T - 1)])
+    left("rel", qbuf.at[pl.ds(0, K - 1)])
+    left("acc", accs)
+    left("ml", mls)
+    left("o", osend.at[pl.ds(0, T - 1)])
+    left("early", eas.at[pl.ds(0, K - 1)])
+    left("h", h3.at[pl.ds(0, K - 1)])
+
+    @pl.when(owner)
+    def _():
+        left("es", es.at[pl.ds(0, K - 1)])
+        left("ab", er.at[pl.ds(0, T - 1)])
+
+    @pl.when(jnp.logical_not(owner))
+    def _():
+        left("es", es)
+
+    left("gu", gus.at[pl.ds(0, K - 1)])
+    left("sm", sms.at[pl.ds(0, K - 1)])
+    left("hb", hb.at[pl.ds(0, K - 1)])
+    left("ps", psb.at[pl.ds(0, K - 1)])
+    arrive("ls", lr.at[pl.ds(0, T - 1)])
     lowered = sum(lr[s].astype(F32) for s in range(T))
     out[...] = (mid_own + lowered).astype(BF16)
-    for copy in sent:
-        copy.wait_send()
+    left("ls", ls.at[pl.ds(0, T - 1)])
 
 
 def hand_over(a, b, c, a_out, b_out, c_out):
@@ -534,17 +626,18 @@
 
     LW = LAT + 128
     slabs = fl(W // 128, B, 128)
-    scratch = [held(a) for a in big] + [
+    gains = pltpu.VMEM((W // 128, 128), BF16)
+    scratch = [
+        gains, bf(LAT // 128, 128), gains, gains, fl(*cos.shape), fl(*sin.shape),
+    ] + [held(a) for a in big] + [
         bf(T, R, W), slabs, bf(K, T, QN + QR), bf(K, T, QN + QR), fl(K, T, 128), fl(K, T, 128),
-        fl(R, LW), fl(K, R, LW), bf(T, HD, LW), bf(K, T, HD, LW), bf(K, H, LAT), bf(K, H, LAT),
-        fl(K, H, 128), fl(K, H, 128), fl(R, LAT), fl(R, 128), bf(T, HD, LAT), bf(T, HD, LAT),
-        fl(T, HV), bf(K, T, HV), slabs, bf(T, R, W), bf(T, R, W), bf(T, R, W),
-        fl(R, 128), fl(K, T, R, 128), fl(B, 128), slabs, slabs,
-        bf(K, T, FD), bf(K, T, FD), bf(K, T, FD), bf(K, T, FD), fl(K, T, 128), fl(K, T, 128),
-        bf(K, T, FD), bf(T, R, W), bf(T, R, W),
+        fl(R, LW), fl(K, R, LW), bf(T, HD, LW), bf(K, T, HD, LW), bf(K - 1, H, LAT), bf(K, H, LAT),
+        fl(K - 1, 8, 2 * H), fl(K, 8, 2 * H), fl(R, LAT), fl(R, 128), bf(T, HD, LAT), bf(T, HD, LAT),
+        fl(T, HV), bf(K, T, HV), bf(K, T, W), bf(T, T, W), bf(K, T, W), slabs, slabs,
+        bf(K, 2, T, FD), bf(K, 2, T, FD), fl(2, T, FD), bf(K, 2, T, FD), bf(K, 2, T, FD),
+        fl(K, T, 128), fl(K, T, 128), bf(K, T, FD), fl(K, T, 128), bf(T, R, W), bf(T, R, W),
         fl(*key_flat.shape), bf(LAT, QN), bf(LAT, HV),
     ]
-    count = 10 * (K - 1) + 5 * (T - 1) + 2 * (K * T - 1) + 8
     vmem = pl.BlockSpec(memory_space=pltpu.VMEM)
     hbm = pl.BlockSpec(memory_space=pl.ANY)
     out_shape = (
@@ -553,14 +646,16 @@
         jax.ShapeDtypeStruct((R, ROPE), BF16),
     )
     made = pl.pallas_call(
-        functools.partial(layer_kernel, K, T, context),
+        functools.partial(layer_kernel, K, T),
         out_shape=out_shape,
-        in_specs=[vmem] * 7 + [hbm] * len(big),
+        in_specs=[hbm] * (7 + len(big)),
         out_specs=(vmem, vmem, vmem),
         scratch_shapes=scratch + [
-            pltpu.SemaphoreType.DMA((len(big),)),
-            pltpu.SemaphoreType.DMA((count,)),
-            pltpu.SemaphoreType.DMA((count,)),
+            pltpu.SemaphoreType.DMA((7 + len(big),)),
+            pltpu.SemaphoreType.DMA((len(PHASES),)),
+            pltpu.SemaphoreType.DMA((len(PHASES),)),
+            pltpu.SemaphoreType.DMA((T,)),
+            pltpu.SemaphoreType.DMA((K - 1,)),
         ],
         compiler_params=pltpu.CompilerParams(
             collective_id=0, has_side_effects=True, vmem_limit_bytes=60 * 1024 * 1024
@@ -577,7 +672,7 @@
 def layer(*args):
     resid, key_up = args[0], args[7]
     kv, tp = lax.axis_size("kv"), lax.axis_size("tp")
-    if resid.shape[0] == kv and key_up.shape[1] == 8 and tp == 8 and resid.shape[1] % 128 == 0:
+    if kv == 4 and resid.shape[0] == 4 and key_up.shape[1] == 8 and tp == 8 and resid.shape[1] % 128 == 0:
         return fused(*args)
     return body(*args)
 

time: 67.2 us -> 59.1 us (0.88)
  Pallas kernels: 66.3 us -> 58.2 us
    pallas_call x1, Pallas kernels: 65 us -> 56.9 us  [fused(): pl.pallas_call(functools.partial(layer_kernel, K, T), out_shape=out_shape...]
where the time goes in v1:
time: 59.1 us; the launch traced here: 58.9 us
  Pallas kernels  58.2 us (98%)
  between operations  0.65 us (1%)
    pallas_call x1, Pallas kernels, fused(): pl.pallas_call(functools.partial(layer_kernel, K, T), out_shape=out_shape...  56.9 us
    pallas_call x1, Pallas kernels, fused(): pl.pallas_call(hand_over, out_shape=out_shape, in_specs=[vmem] * 3, out_s...  1.31 us

profile of v1, /device:TPU:0, one launch (start us, length us, event | category | flops | bytes accessed | tf_op | source)
XLA Modules:
  0.0 58.9 jit_solution(8904499957371717042)
XLA Ops:
  0.6 56.9 %shard_map.202 = (bf16[4,1024]{1,0:T(4,128)(2,1)}, bf16[4,512]{1,0:T(4,128)(2,1)}, bf16[4,64]{1,0:T(4,128)(2,1)}) custom-call(bf16[4,1024]{1,0:T(4,128)(2,1)} %h_x.1, bf16[32,128]{1,0:T(8,128)(2,1)} %bitcast.16, bf16[4,128]{1,0:T(4,128)(2,1)} %bitcast.19, bf16[32,128]{1,0:T(8,128)(2,1)} %bitcast.17, bf16[32,128]{1,0:T(8,128)(2,1)} %bitcast.18, ...), custom_call_target="tpu_custom_call" | custom-call | tf_op jit(solution)/shard_map/pallas_call | solution.py:648
  57.6 1.3 %shard_map.203 = (bf16[4,1024]{1,0:T(4,128)(2,1)}, bf16[4,512]{1,0:T(4,128)(2,1)}, bf16[4,64]{1,0:T(4,128)(2,1)}) custom-call(bf16[4,1024]{1,0:T(4,128)(2,1)} %get-tuple-element.6.a, bf16[4,512]{1,0:T(4,128)(2,1)} %get-tuple-element.7.b, bf16[4,64]{1,0:T(4,128)(2,1)} %get-tuple-element.8.c), custom_call_target="tpu_custom_call" | custom-call | tf_op jit(solution)/shard_map/pallas_call | solution.py:667

commit v2 on v1

--- a/solution.py
+++ b/solution.py
@@ -212,7 +212,7 @@
     wqn, wqr, wlat, wkr, ku, vu, wo, wg, wu, wd, cl, cr,
     xbuf, xf, qs, qrv, sqs, sqr, lats, latr, qe, qbuf, accs, accr, mls, mlr,
     nls, nks, osend, obuf, ohs, h3, es, er, ab, attf, tall,
-    eas, ear, easum, gus, gur, sms, smr, hb, psb, ls, lr, wide_ref, kus, vus,
+    eas, ear, easum, gus, gur, sms, smr, hb, psb, ls, lr, wide_ref, kus, vus, wgt, wut, clt,
     lsem, ssem, rsem, qsem, relsem,
 ):
     k = lax.axis_index("kv")
@@ -303,11 +303,19 @@
         g = ref[...].astype(F32)
         return jnp.concatenate([g[i:i + 1] for i in range(g.shape[0])], axis=1)
 
-    def by_head(src, dst):
+    def by_head(src, dst, turned=False):
         n = src.shape[1]
         wide_ref[...] = src[...].astype(F32)
         for h in range(HD):
-            dst[:, h * n:(h + 1) * n] = wide_ref[pl.ds(h, LAT, stride=HD), :].astype(BF16)
+            block = wide_ref[pl.ds(h, LAT, stride=HD), :].astype(BF16)
+            if turned:
+                dst[h * n:(h + 1) * n, :] = block.T
+            else:
+                dst[:, h * n:(h + 1) * n] = block
+
+    def turn_over(src, dst):
+        for c in range(0, src.shape[1], 128):
+            dst[c:c + 128, :] = src[:, c:c + 128].T
 
     loads["x"].wait()
     pl.semaphore_wait(barrier, len(tps) + len(kvs))
@@ -328,19 +336,20 @@
     for kk in kvs:
         send("lat", lats, latr.at[k], (kk, t))
     loads["ku"].wait()
-    by_head(ku, kus)
+    by_head(ku, kus, True)
     arrive("x", xbuf.at[pl.ds(0, T - 1)])
     for s in range(T):
         put_rows(xf, s, xbuf[s].astype(F32))
     x = all_rows(xf)
     normed = (x * again).astype(BF16)
     sqs[...] = jnp.broadcast_to(jnp.sum(x * x, axis=1, keepdims=True), (B, 128)).reshape(K, T, 128)
-    loads["qn"].wait()
-    qs[:, :, :QN] = dot(normed, wqn).reshape(K, T, QN).astype(BF16)
-    loads["qr"].wait()
-    qs[:, :, QN:] = dot(normed, wqr).reshape(K, T, QR).astype(BF16)
+    for name, w, n, size in (("qn", wqn, 0, QN), ("qr", wqr, QN, QR)):
+        part = pl.ds(n, size)
+        loads[name].wait()
+        qs[:, :, part] = dot(normed, w).reshape(K, T, size).astype(BF16)
+        for kk in kvs:
+            send("q", qs.at[kk, :, part], qrv.at[k, :, part], (kk, t))
     for kk in kvs:
-        send("q", qs.at[kk], qrv.at[k], (kk, t))
         send("sq", sqs.at[kk], sqr.at[k], (kk, t))
     qrv[pl.ds(k, 1)] = qs[pl.ds(k, 1)]
     sqr[pl.ds(k, 1)] = sqs[pl.ds(k, 1)]
@@ -363,6 +372,9 @@
     nls[...] = new_lat.astype(F32)
     nks[...] = new_key.astype(F32)
 
+    loads["cl"].wait()
+    for r in range(R):
+        turn_over(cl.at[r], clt.at[r])
     arrive("q", qrv.at[pl.ds(0, K - 1)])
     arrive("sq", sqr.at[pl.ds(0, K - 1)])
     q = sum(qrv[s].astype(F32) for s in range(K))
@@ -389,69 +401,87 @@
     qe[:, :, LAT:] = jnp.dot(
         spread(q_rope, ROPE), fold, preferred_element_type=F32
     ).reshape(T, HD, RP).astype(BF16)
-    qe[:, :, :LAT] = dot_nt(spread(q_nope, NOPE), kus[...]).reshape(T, HD, LAT).astype(BF16)
+    qe[:, :, :LAT] = dot(spread(q_nope, NOPE), kus).reshape(T, HD, LAT).astype(BF16)
     for tt in tps:
         send("qe", qe.at[tt], qbuf.at[k, t], (k, tt), qsem.at[t])
+    HALF = T // 2
+    near_start = HALF * lax.div(t, HALF)
+    starts = (near_start, HALF - near_start)
     for i, kk in enumerate(kvs):
-        send("rel", qe.at[t], qbuf.at[k, t], (kk, t), relsem.at[i])
+        send("rel", qe.at[t], qbuf.at[k, t], (kk, t), relsem.at[0, i])
     qbuf[pl.ds(k, 1), pl.ds(t, 1)] = qe[pl.ds(t, 1)][None]
-    for tt in by_arrival:
+    for n, tt in enumerate(by_arrival):
         slot = qbuf.at[k, tt]
         settle(slot, qsem.at[tt])
         for i, kk in enumerate(kvs):
-            send("rel", slot, slot, (kk, t), relsem.at[i])
-    loads["cl"].wait()
+            send("rel", slot, slot, (kk, t), relsem.at[int(n >= HALF - 1), i])
     loads["cr"].wait()
 
-    def attend(b):
-        qb32 = qbuf[pl.ds(b, 1)][0].astype(F32).reshape(H, LAT + RP)
-        qb = qb32.astype(BF16)
-        keys = cl[pl.ds(b, 1)][0]
-        scores = (
-            dot_nt(qb[:, :LAT], keys) + jnp.dot(
-                qb[:, LAT:LAT + ROPE], cr[pl.ds(b, 1)][0], preferred_element_type=F32
-            )
-        ) * score_scale
-        m = jnp.max(scores, axis=1, keepdims=True)
-        p = jnp.exp(scores - m)
-        total = jnp.sum(p, axis=1, keepdims=True)
-        acc = jnp.dot(p.astype(BF16), keys, preferred_element_type=F32).astype(BF16)
-        turned_ml = jnp.where(lane_iota((H, 2 * H)) < H, m, total).T
-        return qb32, acc, turned_ml[:1], turned_ml[H:H + 1]
-
-    own_qb, acc, m_row, total_row = attend(k)
+    def as_row(v, shift):
+        shape = (v.shape[0], 2 * H)
+        at = lax.broadcasted_iota(jnp.int32, shape, 0) + shift
+        return jnp.sum(jnp.where(lane_iota(shape) % H == at, v, 0.0), axis=0, keepdims=True)
+
+    def attend(blocks, start, count):
+        wide_qs = [
+            qbuf[pl.ds(b, 1), pl.ds(start, count)][0].astype(F32).reshape(count * HD, LAT + RP)
+            for b in blocks
+        ]
+        narrow = [q32.astype(BF16) for q32 in wide_qs]
+        scores = [
+            (
+                jnp.dot(q16[:, :LAT], clt[pl.ds(b, 1)][0], preferred_element_type=F32)
+                + jnp.dot(q16[:, LAT:LAT + ROPE], cr[pl.ds(b, 1)][0], preferred_element_type=F32)
+            ) * score_scale
+            for q16, b in zip(narrow, blocks)
+        ]
+        tops = [jnp.max(v, axis=1, keepdims=True) for v in scores]
+        probs = [jnp.exp(v - m) for v, m in zip(scores, tops)]
+        accs_of = [
+            jnp.dot(p.astype(BF16), cl[pl.ds(b, 1)][0], preferred_element_type=F32).astype(BF16)
+            for p, b in zip(probs, blocks)
+        ]
+        lanes = lane_iota((count * HD, 2 * H))
+        ml_rows = [
+            as_row(jnp.where(lanes < H, m, jnp.sum(p, axis=1, keepdims=True)), start * HD)
+            for m, p in zip(tops, probs)
+        ]
+        return wide_qs, accs_of, ml_rows
+
+    (own_qb,), (acc,), (ml,) = attend([k], 0, T)
     accr[pl.ds(k, 1)] = acc[None]
-    mlr[pl.ds(k, 1), 0:1, :H] = m_row[None]
-    mlr[pl.ds(k, 1), 1:2, :H] = total_row[None]
+    mlr[pl.ds(k, 1), 0, 0:1, :] = ml[None]
+    mlr[pl.ds(k, 1), 1, 0:1, :] = jnp.zeros_like(ml)[None]
     nl = nls[pl.ds(k, 1), :]
     nk = nks[pl.ds(k, 1), :]
-    own_score = (
+    own_score = as_row((
         jnp.sum(own_qb[:, :LAT] * nl, axis=1, keepdims=True)
         + jnp.sum(own_qb[:, LAT:] * nk, axis=1, keepdims=True)
-    ) * score_scale
-    for i, kk in ((1, kvs[1]), (2, kvs[2]), (0, kvs[0])):
-        settle(qbuf.at[kk], relsem.at[i])
-        _, acc, m_row, total_row = attend(kk)
-        mls[i, 0:1, :H] = m_row
-        mls[i, 1:2, :H] = total_row
-        accs[i] = acc
-        send("acc", accs.at[i], accr.at[k], (kk, t))
-        send("ml", mls.at[i], mlr.at[k], (kk, t))
+    ) * score_scale, 0)
+    for part, start in enumerate(starts):
+        for i, kk in enumerate(kvs):
+            settle(qbuf.at[kk, pl.ds(start, HALF)], relsem.at[part, i])
+        _, part_accs, part_mls = attend(kvs, start, HALF)
+        heads = pl.ds(pl.multiple_of(start * HD, HALF * HD), HALF * HD)
+        for i, kk in enumerate(kvs):
+            mls[i, part, 0:1, :] = part_mls[i]
+            send("ml", mls.at[i, part], mlr.at[k, part], (kk, t))
+        for i, kk in enumerate(kvs):
+            accs[i, part] = part_accs[i]
+            send("acc", accs.at[i, part], accr.at[k, heads], (kk, t))
     arrive("ml", mlr.at[pl.ds(0, K - 1)])
+    peaks = jnp.concatenate([mlr[s, 0, 0:1, :] + mlr[s, 1, 0:1, :] for s in range(K)], axis=0)
+    peak = jnp.maximum(jnp.max(peaks, axis=0, keepdims=True), own_score)
+    share = jnp.exp(peaks - peak)
+    own_prob = jnp.exp(own_score - peak)
+    total = own_prob + jnp.sum(share * pltpu.roll(peaks, H, 1), axis=0, keepdims=True)
+    own_share = jnp.broadcast_to(own_prob / total, (8 - K, 2 * H))
+    columns = jnp.concatenate([share / total, own_share], axis=0).T[:H]
     arrive("acc", accr.at[pl.ds(0, K - 1)])
-    columns = mlr[...].reshape(K * mlr.shape[1], mlr.shape[2]).T[:H]
-    peaks = [columns[:, 8 * s:8 * s + 1] for s in range(K)]
-    peak = own_score
-    for m in peaks:
-        peak = jnp.maximum(peak, m)
-    own_prob = jnp.exp(own_score - peak)
-    total = own_prob
-    summed = own_prob * nl
+    summed = columns[:, K:K + 1] * nl
     for s in range(K):
-        w = jnp.exp(peaks[s] - peak)
-        total = total + w * columns[:, 8 * s + 1:8 * s + 2]
-        summed = summed + w * accr[s].astype(F32)
-    osend[...] = (summed / total).reshape(T, HD, LAT).astype(BF16)
+        summed = summed + columns[:, s:s + 1] * accr[s].astype(F32)
+    osend[...] = summed.reshape(T, HD, LAT).astype(BF16)
     for tt in tps:
         send("o", osend.at[tt], obuf.at[t], (k, tt))
     obuf[pl.ds(t, 1)] = osend[pl.ds(t, 1)]
@@ -475,19 +505,24 @@
     h3[pl.ds(k, 1)] = ohs[...].astype(BF16)[None]
     for kk in kvs:
         send("h", h3.at[k], h3.at[k], (kk, t))
+    turn_over(wu, wut)
     loads["wo"].wait()
     arrive("h", h3.at[pl.ds(0, K - 1)])
-    es[...] = dot(h3[...].astype(F32).reshape(B, HD * VD).astype(BF16), wo).reshape(K, T, W).astype(BF16)
-    first = (T - K) // 2
-    mine = t - first
-    owner = jnp.logical_and(mine >= 0, mine < K)
-    for i in range(K):
-        j = lax.rem(i + (K // 2) * (1 - lax.div(t, T // 2)), K)
-
-        @pl.when(mine != j)
+    OWNERS, share_rows = es.shape[0], es.shape[1]
+    es[...] = dot(
+        h3[...].astype(F32).reshape(B, HD * VD).astype(BF16), wo
+    ).reshape(OWNERS, share_rows, W).astype(BF16)
+    owners = (T // 2 - 1, T // 2 + 1)
+    mine = lax.div(t, T // 2)
+    owner = lax.rem(t + 1, T) == mine * 2 + T // 2
+    for i in range(OWNERS):
+        j = lax.rem(i + 1 + mine, OWNERS)
+
+        @pl.when(jnp.logical_not(jnp.logical_and(owner, mine == j)))
         def _():
-            send("es", es.at[j], er.at[t], (k, first + j))
-
+            send("es", es.at[j], er.at[t], (k, 2 * j + owners[0]))
+
+    turn_over(wg, wgt)
     arrive("early", ear.at[pl.ds(0, K - 1)])
     easum[...] = sum(ear[s].astype(F32) for s in range(K))
     loads["pg"].wait()
@@ -499,7 +534,7 @@
         ab[pl.ds(mine, 1)] = sum(er[s].astype(F32) for s in range(T)).astype(BF16)[None]
         for tt in tps:
             send("ab", ab.at[mine], ab.at[mine], (k, tt))
-        arrive("ab", ab.at[pl.ds(0, K - 1)])
+        arrive("ab", ab.at[pl.ds(0, OWNERS - 1)])
 
     @pl.when(jnp.logical_not(owner))
     def _():
@@ -508,12 +543,6 @@
     att = ab[...].astype(F32).reshape(B, W)
     added = att * gain_row(pg)
     late = (added * gain_row(mg)).astype(BF16)
-    gus[:, 0] = dot_nt(late, wg[...]).reshape(K, T, FD).astype(BF16)
-    for kk in kvs:
-        send("gu", gus.at[kk, 0], gur.at[k, 0], (kk, t))
-    gus[:, 1] = dot_nt(late, wu[...]).reshape(K, T, FD).astype(BF16)
-    for kk in kvs:
-        send("gu", gus.at[kk, 1], gur.at[k, 1], (kk, t))
     lane = lane_iota((B, 128))
     parts = (
         jnp.sum(att * att, axis=1, keepdims=True),
@@ -523,17 +552,24 @@
     sms[...] = jnp.where(
         lane < 32, parts[0], jnp.where(lane < 64, parts[1], parts[2])
     ).reshape(K, T, 128)
-    for kk in kvs:
-        send("sm", sms.at[kk], smr.at[k], (kk, t))
+    cut = (FD // 256 + 1) * 128
+    for i, w, n, size in ((0, wgt, 0, FD), (1, wut, 0, cut), (1, wut, cut, FD - cut)):
+        part = pl.ds(n, size)
+        gus[:, i, :, part] = dot(late, w.at[:, part]).reshape(K, T, size).astype(BF16)
+        for kk in kvs:
+            send("gu", gus.at[kk, i, :, part], gur.at[k, i, :, part], (kk, t))
+        if i == 0:
+            for kk in kvs:
+                send("sm", sms.at[kk], smr.at[k], (kk, t))
     gur[pl.ds(k, 1)] = gus[pl.ds(k, 1)]
     smr[pl.ds(k, 1)] = sms[pl.ds(k, 1)]
     put_all(attf, att)
     arrive("sm", smr.at[pl.ds(0, K - 1)])
-    arrive("gu", gur.at[pl.ds(0, K - 1)])
     sums = sum(smr[s] for s in range(K))
     post_scale = lax.rsqrt(sums[:, :1] / D + EPS)
     mid_square = square + post_scale * (2.0 * sums[:, 32:33] + post_scale * sums[:, 64:65])
     mid_scale = lax.rsqrt(jnp.maximum(mid_square, 0.0) / D + EPS)
+    arrive("gu", gur.at[pl.ds(0, K - 1)])
     gate = (easum[0] + post_scale * sum(gur[s, 0].astype(F32) for s in range(K))) * mid_scale
     up = (easum[1] + post_scale * sum(gur[s, 1].astype(F32) for s in range(K))) * mid_scale
     hb[pl.ds(k, 1)] = (gate / (1.0 + jnp.exp(-gate)) * up).astype(BF16)[None]
@@ -568,7 +604,7 @@
 
     @pl.when(owner)
     def _():
-        left("es", es.at[pl.ds(0, K - 1)])
+        left("es", es.at[pl.ds(0, OWNERS - 1)])
         left("ab", er.at[pl.ds(0, T - 1)])
 
     @pl.when(jnp.logical_not(owner))
@@ -631,23 +667,20 @@
         gains, bf(LAT // 128, 128), gains, gains, fl(*cos.shape), fl(*sin.shape),
     ] + [held(a) for a in big] + [
         bf(T, R, W), slabs, bf(K, T, QN + QR), bf(K, T, QN + QR), fl(K, T, 128), fl(K, T, 128),
-        fl(R, LW), fl(K, R, LW), bf(T, HD, LW), bf(K, T, HD, LW), bf(K - 1, H, LAT), bf(K, H, LAT),
-        fl(K - 1, 8, 2 * H), fl(K, 8, 2 * H), fl(R, LAT), fl(R, 128), bf(T, HD, LAT), bf(T, HD, LAT),
-        fl(T, HV), bf(K, T, HV), bf(K, T, W), bf(T, T, W), bf(K, T, W), slabs, slabs,
+        fl(R, LW), fl(K, R, LW), bf(T, HD, LW), bf(K, T, HD, LW), bf(K - 1, 2, H // 2, LAT), bf(K, H, LAT),
+        fl(K - 1, 2, 8, 2 * H), fl(K, 2, 8, 2 * H), fl(R, LAT), fl(R, 128), bf(T, HD, LAT), bf(T, HD, LAT),
+        fl(T, HV), bf(K, T, HV), bf(2, B // 2, W), bf(T, B // 2, W), bf(2, B // 2, W), slabs, slabs,
         bf(K, 2, T, FD), bf(K, 2, T, FD), fl(2, T, FD), bf(K, 2, T, FD), bf(K, 2, T, FD),
         fl(K, T, 128), fl(K, T, 128), bf(K, T, FD), fl(K, T, 128), bf(T, R, W), bf(T, R, W),
-        fl(*key_flat.shape), bf(LAT, QN), bf(LAT, HV),
+        fl(*key_flat.shape), bf(QN, LAT), bf(LAT, HV), bf(W, FD), bf(W, FD),
+        bf(R, LAT, cache_latent.shape[1]),
     ]
     vmem = pl.BlockSpec(memory_space=pltpu.VMEM)
-    hbm = pl.BlockSpec(memory_space=pl.ANY)
-    out_shape = (
-        jax.ShapeDtypeStruct((R, W), BF16),
-        jax.ShapeDtypeStruct((R, LAT), BF16),
-        jax.ShapeDtypeStruct((R, ROPE), BF16),
-    )
+    hbm = pl.BlockSpec(memory_space=pltpu.HBM)
+    shapes = ((R, W), (R, LAT), (R, ROPE))
     made = pl.pallas_call(
         functools.partial(layer_kernel, K, T),
-        out_shape=out_shape,
+        out_shape=tuple(pltpu.VMEM(shape, BF16) for shape in shapes),
         in_specs=[hbm] * (7 + len(big)),
         out_specs=(vmem, vmem, vmem),
         scratch_shapes=scratch + [
@@ -655,7 +688,7 @@
             pltpu.SemaphoreType.DMA((len(PHASES),)),
             pltpu.SemaphoreType.DMA((len(PHASES),)),
             pltpu.SemaphoreType.DMA((T,)),
-            pltpu.SemaphoreType.DMA((K - 1,)),
+            pltpu.SemaphoreType.DMA((2, K - 1)),
         ],
         compiler_params=pltpu.CompilerParams(
             collective_id=0, has_side_effects=True, vmem_limit_bytes=60 * 1024 * 1024
@@ -665,8 +698,11 @@
         jnp.asarray(cos), jnp.asarray(sin), *big,
     )
     return pl.pallas_call(
-        hand_over, out_shape=out_shape, in_specs=[vmem] * 3, out_specs=(vmem,) * 3
-    )(*made)
+        hand_over,
+        out_shape=tuple(jax.ShapeDtypeStruct(shape, BF16) for shape in shapes),
+        in_specs=[vmem] * 3,
+        out_specs=(vmem,) * 3,
+    )(*(pltpu.with_memory_space_constraint(a, pltpu.VMEM) for a in made))
 
 
 def layer(*args):

time: 59.1 us -> 54.4 us (0.920)
  Pallas kernels: 58.2 us -> 53.5 us
    pallas_call x2, Pallas kernels: 58.2 us -> 53.5 us  [the longest x1 52.9 us: fused(): pl.pallas_call(functools.partial(layer_kernel, K, T), out_shape=tuple((pl...]
where the time goes in v2:
time: 54.4 us; the launch traced here: 54.1 us
  Pallas kernels  53.5 us (98%)
  between operations  0.65 us (1%)
    pallas_call x1, Pallas kernels, fused(): pl.pallas_call(functools.partial(layer_kernel, K, T), out_shape=tuple((pl...  52.9 us

profile of v2, /device:TPU:0, one launch (start us, length us, event | category | flops | bytes accessed | tf_op | source)
XLA Modules:
  0.0 54.1 jit_solution(9442936759320844568)
XLA Ops:
  0.6 52.9 %shard_map.202 = (bf16[4,1024]{1,0:T(4,128)(2,1)S(1)}, bf16[4,512]{1,0:T(4,128)(2,1)S(1)}, bf16[4,64]{1,0:T(4,128)(2,1)S(1)}) custom-call(bf16[4,1024]{1,0:T(4,128)(2,1)} %h_x.1, bf16[32,128]{1,0:T(8,128)(2,1)} %bitcast.16, bf16[4,128]{1,0:T(4,128)(2,1)} %bitcast.19, bf16[32,128]{1,0:T(8,128)(2,1)} %bitcast.17, bf16[32,128]{1,0:T(8,128)(2,1)} %bitcast.18, ...), custom_call_target="tpu_custom_call" | custom-call | tf_op jit(solution)/shard_map/pallas_call | solution.py:681
  53.5 0.6 %shard_map.203 = (bf16[4,1024]{1,0:T(4,128)(2,1)}, bf16[4,512]{1,0:T(4,128)(2,1)}, bf16[4,64]{1,0:T(4,128)(2,1)}) custom-call(bf16[4,1024]{1,0:T(4,128)(2,1)S(1)} %get-tuple-element.6.a, bf16[4,512]{1,0:T(4,128)(2,1)S(1)} %get-tuple-element.7.b, bf16[4,64]{1,0:T(4,128)(2,1)S(1)} %get-tuple-element.8.c), custom_call_target="tpu_custom_call" | custom-call | tf_op jit(solution)/shard_map/pallas_call | solution.py:700
